TPU v7x, 32 devices: a whole 2x2x4 slice. The times are simulated.
32 devices in a mesh: sp: 4 (over y, x), dp: 8 (over z, core).
Axes of the slice: x: 2, y: 2, z: 4, core: 2. Of those that a mesh axis runs over, the one named last changes fastest.
Arguments:
- value_half: bfloat16 [8, 1024, 2048], P('dp', 'sp'), may hold values from -6 to 6
- gate_half: bfloat16 [8, 1024, 2048], P('dp', 'sp'), may hold values from -6 to 6
- upstream: bfloat16 [8, 1024, 2048], P('dp', 'sp'), may hold values from -6 to 6
- conv_taps: float32 [31, 2048], P(None, 'sp'), may hold values from -1 to 1
- norm_gain: float32 [2048], replicated, may hold values from 0.1 to 1.9
- out_weight: bfloat16 [2048, 2048], P('dp'), may hold values from -0.125 to 0.125
Outputs:
- grad_value: bfloat16 [8, 1024, 2048], P('dp', 'sp')
- grad_gate: bfloat16 [8, 1024, 2048], P('dp', 'sp')
- grad_taps: float32 [31, 2048], P(None, 'sp')
- grad_gain: float32 [2048], replicated
- grad_weight: float32 [2048, 2048], P('dp')
All inputs are finite; a program needn't handle non-finite values.
Results may differ from a plain program's by a relative error of at most 0.0062.
Values may be sent and summed in bfloat16 or wider, within the bound.
A program may use at most 128 MiB of HBM per device.

v0:
```python
import jax
import jax.numpy as jnp
from jax import lax
from jax.sharding import PartitionSpec as P

NORM_EPS = 1e-05


def body(value_half, gate_half, upstream, conv_taps, norm_gain, out_weight):
    tap_count = conv_taps.shape[0]
    sig_gate = jax.nn.sigmoid(gate_half.astype(jnp.float32))
    value_wide = value_half.astype(jnp.float32)
    glu = (value_wide * sig_gate).astype(jnp.bfloat16)
    glu_heads = lax.all_to_all(glu, "sp", split_axis=2, concat_axis=1, tiled=True).astype(
        jnp.float32
    )
    length = glu_heads.shape[1]
    padded = jnp.pad(glu_heads, ((0, 0), (tap_count - 1, 0), (0, 0)))
    conv_out = jnp.zeros_like(glu_heads)
    for offset in range(tap_count):
        conv_out = conv_out + conv_taps[offset] * padded[:, offset : offset + length]
    conv_tokens = lax.all_to_all(
        conv_out.astype(jnp.bfloat16), "sp", split_axis=1, concat_axis=2, tiled=True
    ).astype(jnp.float32)
    row_mean = jnp.mean(conv_tokens, axis=-1, keepdims=True)
    centered = conv_tokens - row_mean
    inv_scale = lax.rsqrt(jnp.mean(centered * centered, axis=-1, keepdims=True) + NORM_EPS)
    normed = centered * inv_scale
    scaled = normed * norm_gain
    sig_scaled = jax.nn.sigmoid(scaled)
    activated = (scaled * sig_scaled).astype(jnp.bfloat16)[0]
    upstream_rows = upstream[0]
    columns = upstream_rows
    grad_act = jnp.dot(
        columns,
        lax.all_gather(out_weight, "dp", axis=0, tiled=True),
        preferred_element_type=jnp.float32,
    )
    grad_scaled = grad_act[None] * sig_scaled * (1.0 + scaled * (1.0 - sig_scaled))
    gain_part = jnp.sum(grad_scaled * normed, axis=(0, 1))
    grad_normed = grad_scaled * norm_gain
    grad_conv_out = inv_scale * (
        grad_normed
        - jnp.mean(grad_normed, axis=-1, keepdims=True)
        - normed * jnp.mean(grad_normed * normed, axis=-1, keepdims=True)
    )
    grad_heads = lax.all_to_all(
        grad_conv_out.astype(jnp.bfloat16), "sp", split_axis=2, concat_axis=1, tiled=True
    ).astype(jnp.float32)
    grad_padded = jnp.pad(grad_heads, ((0, 0), (0, tap_count - 1), (0, 0)))
    grad_glu = jnp.zeros_like(grad_heads)
    tap_terms = []
    for offset in range(tap_count):
        first = tap_count - 1 - offset
        grad_glu = grad_glu + conv_taps[offset] * grad_padded[:, first : first + length]
        tap_terms.append(jnp.sum(grad_heads * padded[:, offset : offset + length], axis=(0, 1)))
    grad_taps = lax.psum(jnp.stack(tap_terms), "dp")
    grad_tokens = lax.all_to_all(
        grad_glu.astype(jnp.bfloat16), "sp", split_axis=1, concat_axis=2, tiled=True
    ).astype(jnp.float32)
    grad_value = (grad_tokens * sig_gate).astype(jnp.bfloat16)
    grad_gate = (grad_tokens * value_wide * sig_gate * (1.0 - sig_gate)).astype(jnp.bfloat16)
    grad_gain = lax.psum(gain_part, ("sp", "dp"))
    columns = upstream_rows
    owned = lax.psum_scatter(
        lax.dot_general(
            columns, activated, (((0,), (0,)), ((), ())), preferred_element_type=jnp.float32
        ),
        "dp",
        scatter_dimension=0,
        tiled=True,
    )
    grad_weight = lax.psum(owned, "sp")
    return (grad_value, grad_gate, grad_taps, grad_gain, grad_weight)


def solution(mesh):
    placed = (
        P("dp", "sp", None),
        P("dp", "sp", None),
        P("dp", "sp", None),
        P(None, "sp"),
        P(),
        P("dp", None),
    )
    return jax.shard_map(
        body,
        mesh=mesh,
        in_specs=placed,
        out_specs=(P("dp", "sp", None), P("dp", "sp", None), P(None, "sp"), P(), P("dp", None)),
        check_vma=False,
    )
```

profile of v0, /device:TPU:0, one launch (start us, length us, event | category | flops | bytes accessed | tf_op | source)
XLA Modules:
  0.0 395.5 jit_solution(13518251392995277205)
XLA Ops:
  11.9 12.9 %copy.90 = bf16[1,256,2048]{1,0,2:T(2,128)(2,1)} copy(bf16[1,256,2048]{1,2,0:T(8,128)(2,1)S(1)} %fusion.1) | data formatting | bytes 2097152 | tf_op jit(solution)/shard_map/convert_element_type | solution.py:13
  25.3 11.6 %reduce.17 = bf16[2048,256]{1,0:T(8,128)(2,1)S(1)} reduce(bf16[2048,1,256]{2,1,0:T(2,128)(2,1)} %bitcast.178, bf16[]{:T(256)} %broadcast.201), dimensions={1}, to_apply=%bitcast.161.reduce_sub_computation | reduce | bytes 2097154
  38.6 5.4 %all-to-all-start = ((bf16[4,2,65536]{2,1,0:T(2,128)(2,1)}), bf16[4,2,65536]{2,1,0:T(2,128)(2,1)}, u32[]{:S(2)}, u32[]{:S(2)}) async-start(bf16[4,2,65536]{2,1,0:T(2,128)(2,1)} %reshape.389), calls=%async_computation | async-start | bytes 2097152 | tf_op jit(solution)/shard_map/all_to_all | solution.py:14
  44.1 14.2 %all-to-all-done = bf16[4,2,65536]{2,1,0:T(2,128)(2,1)} async-done(((bf16[4,2,65536]{2,1,0:T(2,128)(2,1)}), bf16[4,2,65536]{2,1,0:T(2,128)(2,1)}, u32[]{:S(2)}, u32[]{:S(2)}) %all-to-all-start) | async-done | bytes 1048608 | tf_op jit(solution)/shard_map/all_to_all | solution.py:14
  64.9 8.0 %add_convert_fusion.1 = bf16[1,1024,512]{2,1,0:T(8,128)(2,1)S(1)} fusion(f32[1,1024,512]{2,1,0:T(8,128)S(1)} %bitcast.163, f32[512]{0:T(512)S(1)} %bitcast.207, f32[512]{0:T(512)S(1)} %bitcast.209, f32[512]{0:T(512)S(1)} %bitcast.213, f32[512]{0:T(512)S(1)} %bitcast.215, f32[512]{0:T(512)S(1)} %bitcast.217, f32[512]{0:T(512)S(1)} %bitcast.219, ...), kind=kLoop, calls=%fused_computation.88 | loop fusion | flops 32505856 | bytes 3209216 | tf_op jit(solution)/shard_map/convert_element_type | solution.py:23
  72.9 2.9 copy.89
  75.8 8.1 %reduce.18 = bf16[1024,512]{1,0:T(8,128)(2,1)S(1)} reduce(bf16[1024,1,512]{2,1,0:T(2,128)(2,1)} %bitcast.180, bf16[]{:T(256)} %broadcast.201), dimensions={1}, to_apply=%bitcast.160.reduce_sub_computation | reduce | bytes 2097154
  85.9 4.3 %all-to-all-start.1 = ((bf16[4,2,65536]{2,1,0:T(2,128)(2,1)}), bf16[4,2,65536]{2,1,0:T(2,128)(2,1)}, u32[]{:S(2)}, u32[]{:S(2)}) async-start(bf16[4,2,65536]{2,1,0:T(2,128)(2,1)} %reshape.391), calls=%async_computation.1 | async-start | bytes 2097152 | tf_op jit(solution)/shard_map/all_to_all | solution.py:22
  90.2 13.4 %all-to-all-done.1 = bf16[4,2,65536]{2,1,0:T(2,128)(2,1)} async-done(((bf16[4,2,65536]{2,1,0:T(2,128)(2,1)}), bf16[4,2,65536]{2,1,0:T(2,128)(2,1)}, u32[]{:S(2)}, u32[]{:S(2)}) %all-to-all-start.1) | async-done | bytes 1048608 | tf_op jit(solution)/shard_map/all_to_all | solution.py:22
  103.6 3.0 reshape.392
  117.6 9.3 %convolution_bitcast_fusion = f32[2048,2048]{0,1:T(8,128)} fusion(bf16[256,2048]{0,1:T(8,128)(2,1)} %bitcast.186, bf16[1,256,2048]{2,1,0:T(8,128)(2,1)S(1)} %copy-done), kind=kOutput, calls=%fused_computation | convolution fusion | flops 2147483648 | bytes 18874368 | tf_op jit(solution)/shard_map/dot_general | solution.py:66
  129.2 5.7 %multiply_reduce_fusion = (f32[2048]{0:T(1024)S(1)}, f32[256]{0:T(256)S(1)}, f32[256]{0:T(256)S(1)}, f32[256,2048]{1,0:T(8,128)S(1)}) fusion(f32[256,2048]{1,0:T(8,128)S(1)} %bitcast.176, f32[256]{0:T(256)S(1)} %broadcast_multiply_fusion.2, f32[256]{0:T(256)S(1)} %add_rsqrt_fusion, f32[2048]{0:T(1024)S(1)} %copy-done.11, ...), kind=kOutput, calls=%fused_computation.20 | convolution fusion | flops 2156393984 | bytes 13651968 | tf_op jit(solution)/shard_map/dot_general | solution.py:34
  137.4 10.8 %reduce.19 = bf16[2048,256]{1,0:T(8,128)(2,1)S(1)} reduce(bf16[2048,1,256]{2,1,0:T(2,128)(2,1)S(1)} %bitcast.182, bf16[]{:T(256)} %broadcast.201), dimensions={1}, to_apply=%bitcast.148.reduce_sub_computation | reduce | bytes 2097154
  149.8 3.5 all-to-all-start.2
  153.4 48.8 %psum.22 = f32[2048]{0:T(1024)} all-reduce(f32[2048]{0:T(1024)S(1)} %get-tuple-element.35), channel_id=1, replica_groups=mesh['sp'=4,'dp'=8] {'sp','dp'}, use_global_device_ids=true, to_apply=%region_39.40 | all-reduce | flops 2048 | bytes 16384 | tf_op jit(solution)/shard_map/psum | solution.py:63
  207.1 8.0 %add_convert_fusion = bf16[1,1024,512]{2,1,0:T(8,128)(2,1)S(1)} fusion(f32[1,1024,512]{2,1,0:T(8,128)S(1)} %bitcast.162, f32[512]{0:T(512)S(1)} %bitcast.208, f32[512]{0:T(512)S(1)} %bitcast.210, f32[512]{0:T(512)S(1)} %bitcast.214, f32[512]{0:T(512)S(1)} %bitcast.216, f32[512]{0:T(512)S(1)} %bitcast.218, f32[512]{0:T(512)S(1)} %bitcast.220, ...), kind=kLoop, calls=%fused_computation.52 | loop fusion | flops 32505856 | bytes 3209216 | tf_op jit(solution)/shard_map/convert_element_type | solution.py:59
  215.0 81.4 %reduce-scatter.2.cloned.1.call-done = f32[256,2048]{0,1:T(8,128)} async-done(((f32[2048,2048]{0,1:T(8,128)}), f32[256,2048]{0,1:T(8,128)}) %reduce-scatter.2.cloned.1.call-update) | async-done | bytes 2097168 | tf_op jit(solution)/shard_map/reduce_scatter | solution.py:65
  296.5 17.9 %multiply_reduce_fusion.2 = (f32[512]{0:T(512)S(1)}, f32[512]{0:T(512)S(1)}, f32[512]{0:T(512)S(1)}, f32[512]{0:T(512)S(1)}, f32[512]{0:T(512)S(1)}, /*index=5*/...) fusion(f32[1,1024,512]{2,1,0:T(8,128)} %bitcast.164, ...), kind=kLoop, calls=%fused_computation.22 | loop fusion | flops 18865152 | bytes 4231168 | tf_op jit(solution)/shard_map/reduce_sum | solution.py:56
  317.4 8.0 %reduce.20 = bf16[1024,512]{1,0:T(8,128)(2,1)S(1)} reduce(bf16[1024,1,512]{2,1,0:T(2,128)(2,1)} %bitcast.179, bf16[]{:T(256)} %broadcast.201), dimensions={1}, to_apply=%bitcast.159.reduce_sub_computation | reduce | bytes 2097154
  327.4 3.7 all-to-all-start.3
  333.7 11.8 %multiply_reduce_fusion.3 = (f32[512]{0:T(512)S(1)}, f32[512]{0:T(512)S(1)}, f32[512]{0:T(512)S(1)}, f32[512]{0:T(512)S(1)}, f32[512]{0:T(512)S(1)}, /*index=5*/...) fusion(f32[1,1024,512]{2,1,0:T(8,128)} %bitcast.165, ...), kind=kLoop, calls=%fused_computation.23 | loop fusion | flops 12576768 | bytes 4218880 | tf_op jit(solution)/shard_map/reduce_sum | solution.py:56
  345.7 27.2 %psum.21 = f32[31,512]{1,0:T(8,128)} all-reduce(f32[31,512]{1,0:T(8,128)S(1)} %stack.127), channel_id=1, replica_groups=mesh['sp'=4,'dp'=8] {'dp'}, use_global_device_ids=true, to_apply=%region_37.38 | all-reduce | flops 15872 | bytes 126976 | tf_op jit(solution)/shard_map/psum | solution.py:57
  375.7 3.0 copy.70
  378.8 3.4 fusion.4
  (77 shorter events, 54.9 us)
Async XLA Ops:
  7.2 110.5 %copy-start = (bf16[1,256,2048]{2,1,0:T(8,128)(2,1)S(1)}, bf16[1,256,2048]{2,1,0:T(8,128)(2,1)}, u32[]{:S(2)}) copy-start(bf16[1,256,2048]{2,1,0:T(8,128)(2,1)} %param.8) | copy-start | bytes 3145732
  7.2 122.0 %all-gather.2.cloned.1.call-start = ((), (), s32[]{:S(2)}) async-start(), calls=%async_computation.5 | async-start | bytes 9437184 | tf_op jit(solution)/shard_map/all_gather | solution.py:36
  9.4 2.5 copy-start.6
  11.3 13.5 %copy-start.8 = (bf16[1,256,2048]{1,2,0:T(8,128)(2,1)}, bf16[1,256,2048]{1,2,0:T(8,128)(2,1)S(1)}, u32[]{:S(2)}) copy-start(bf16[1,256,2048]{1,2,0:T(8,128)(2,1)S(1)} %copy.57) | copy-start | bytes 3145732
  37.0 7.1 %copy-start.10 = (f32[31,512]{1,0:T(8,128)S(1)}, f32[31,512]{1,0:T(8,128)}, u32[]{:S(2)}) copy-start(f32[31,512]{1,0:T(8,128)} %param.9) | copy-start | bytes 190468
  38.6 19.7 %all-to-all-start = ((bf16[4,2,65536]{2,1,0:T(2,128)(2,1)}), bf16[4,2,65536]{2,1,0:T(2,128)(2,1)}, u32[]{:S(2)}, u32[]{:S(2)}) async-start(bf16[4,2,65536]{2,1,0:T(2,128)(2,1)} %reshape.389), calls=%async_computation | async-start | bytes 2097152 | tf_op jit(solution)/shard_map/all_to_all | solution.py:14
  60.9 2.0 copy-start.3
  64.9 10.9 %copy-start.2 = (f32[1,4,256,512]{3,2,1,0:T(8,128)}, f32[1,4,256,512]{3,2,1,0:T(8,128)S(1)}, u32[]{:S(2)}) copy-start(f32[1,4,256,512]{3,2,1,0:T(8,128)S(1)} %copy.60) | copy-start | bytes 6291460
  83.9 6.3 %copy-start.11 = (f32[2048]{0:T(1024)S(1)}, f32[2048]{0:T(1024)}, u32[]{:S(2)}) copy-start(f32[2048]{0:T(1024)} %param.10) | copy-start | bytes 24580
  85.9 17.7 %all-to-all-start.1 = ((bf16[4,2,65536]{2,1,0:T(2,128)(2,1)}), bf16[4,2,65536]{2,1,0:T(2,128)(2,1)}, u32[]{:S(2)}, u32[]{:S(2)}) async-start(bf16[4,2,65536]{2,1,0:T(2,128)(2,1)} %reshape.391), calls=%async_computation.1 | async-start | bytes 2097152 | tf_op jit(solution)/shard_map/all_to_all | solution.py:22
  90.2 206.3 %reduce-scatter.2.cloned.1.call-start = ((), (), s32[]{:S(2)}) async-start(), calls=%async_computation.6 | async-start | bytes 18874368 | tf_op jit(solution)/shard_map/reduce_scatter | solution.py:65
  106.6 1.3 copy-start.5
  149.8 52.3 %all-to-all-start.2 = ((bf16[4,2,65536]{2,1,0:T(2,128)(2,1)}), bf16[4,2,65536]{2,1,0:T(2,128)(2,1)S(1)}, u32[]{:S(2)}, u32[]{:S(2)}) async-start(bf16[4,2,65536]{2,1,0:T(2,128)(2,1)} %reshape.393), calls=%async_computation.2 | async-start | bytes 2097152 | tf_op jit(solution)/shard_map/all_to_all | solution.py:47
  153.3 232.5 %all-reduce.4.cloned.1.call-start = ((), (), s32[]{:S(2)}) async-start(), calls=%async_computation.7 | async-start | bytes 4194304 | tf_op jit(solution)/shard_map/psum | solution.py:73
  203.1 2.0 copy-start.4
  327.4 45.5 %all-to-all-start.3 = ((bf16[4,2,65536]{2,1,0:T(2,128)(2,1)}), bf16[4,2,65536]{2,1,0:T(2,128)(2,1)S(1)}, u32[]{:S(2)}, u32[]{:S(2)}) async-start(bf16[4,2,65536]{2,1,0:T(2,128)(2,1)} %reshape.395), calls=%async_computation.3 | async-start | bytes 2097152 | tf_op jit(solution)/shard_map/all_to_all | solution.py:58
  375.7 3.0 copy-start.7
  375.7 3.0 copy-start.9
  384.4 4.3 %copy-start.1 = (bf16[1,256,2048]{2,1,0:T(8,128)(2,1)S(1)}, bf16[1,256,2048]{2,1,0:T(8,128)(2,1)}, u32[]{:S(2)}) copy-start(bf16[1,256,2048]{2,1,0:T(8,128)(2,1)} %param.8) | copy-start | bytes 3145732
Sparse Core Ops, SparseCore 0:
  9.6 84.7 all-gather.1
  127.1 169.3 reduce-scatter.1
  299.6 69.1 all-reduce.3
where the time goes:
time: 402 us; the launch traced here: 395 us
  waiting for transfers between devices  110 us (27%)
  other arithmetic  102 us (25%)
  blocking collectives  75.9 us (19%)
  local copies, waits for them, and re-layouts  61.5 us (15%)
  starting transfers between devices  16.9 us (4%)
  matrix products  15 us (4%)
  between operations  14.3 us (4%)
    reduce_scatter x1, waiting for transfers between devices, body(): lax.psum_scatter(lax.dot_general(columns, activated, (((0,), (0,)), ((),...  81.4 us
    psum x1, blocking collectives, body(): grad_gain = lax.psum(gain_part, ('sp', 'dp'))  48.8 us
    unnamed x4, other arithmetic  38.5 us
    reduce_sum x4, other arithmetic, body(): jnp.sum(grad_heads * padded[:, offset:offset + length], axis=(0, 1))  32.4 us
    unnamed x39, local copies, waits for them, and re-layouts  28.2 us
    psum x1, blocking collectives, body(): grad_taps = lax.psum(jnp.stack(tap_terms), 'dp')  27.2 us
    all_to_all x1, waiting for transfers between devices, body(): lax.all_to_all(glu, 'sp', split_axis=2, concat_axis=1, tiled=True)  14.2 us
    all_to_all x1, waiting for transfers between devices, body(): lax.all_to_all(conv_out.astype(jnp.bfloat16), 'sp', split_axis=1, concat_...  13.4 us
  transfers between devices with their start and end apart: 7, of which 3 were waited for; matrix products, arithmetic and copies ran while one was open for 44% of the time, Pallas kernels for 0%

commit v1 on v0

--- a/solution.py
+++ b/solution.py
@@ -60,7 +60,7 @@
     ).astype(jnp.float32)
     grad_value = (grad_tokens * sig_gate).astype(jnp.bfloat16)
     grad_gate = (grad_tokens * value_wide * sig_gate * (1.0 - sig_gate)).astype(jnp.bfloat16)
-    grad_gain = lax.psum(gain_part, ("sp", "dp"))
+    grad_gain = lax.psum(lax.psum(gain_part, axis_name="sp"), axis_name="dp")
     columns = upstream_rows
     owned = lax.psum_scatter(
         lax.dot_general(

time: 402 us -> 443 us (1.10)
  waiting for transfers between devices: 110 us -> 206 us
  blocking collectives: 75.9 us -> 17 us
  local copies, waits for them, and re-layouts: 61.5 us -> 66.5 us
    psum x2 -> x1, blocking collectives: 75.9 us -> 17 us  [body(): grad_gain = lax.psum(lax.psum(gain_part, axis_name='sp'), axis_name='dp')]
    psum x0 -> x1, waiting for transfers between devices: none -> 50.3 us  [body(): grad_taps = lax.psum(jnp.stack(tap_terms), 'dp')]
    reduce_scatter x1, waiting for transfers between devices: 81.4 us -> 120 us  [body(): lax.psum_scatter(lax.dot_general(columns, activated, (((0,), (0,)), ((),...]
    psum x1, waiting for transfers between devices: 0.01 us -> 7.13 us  [body(): grad_weight = lax.psum(owned, 'sp')]
    unnamed x39 -> x45, local copies, waits for them, and re-layouts: 28.2 us -> 30.8 us
  transfers between devices with their start and end apart: 7 -> 8, of which waited for: 3 -> 5; matrix products, arithmetic and copies ran while one was open for 44% -> 41% of each run, Pallas kernels for 0% -> 0%
where the time goes in v1:
time: 443 us; the launch traced here: 436 us
  waiting for transfers between devices  206 us (47%)
  other arithmetic  100 us (23%)
  local copies, waits for them, and re-layouts  66.5 us (15%)
  starting transfers between devices  17 us (4%)
  blocking collectives  17 us (4%)
  matrix products  15 us (3%)
  between operations  14.3 us (3%)
    reduce_scatter x1, waiting for transfers between devices, body(): lax.psum_scatter(lax.dot_general(columns, activated, (((0,), (0,)), ((),...  120 us
    psum x1, waiting for transfers between devices, body(): grad_taps = lax.psum(jnp.stack(tap_terms), 'dp')  50.3 us
    unnamed x4, other arithmetic  38.8 us
    unnamed x45, local copies, waits for them, and re-layouts  30.8 us
    reduce_sum x4, other arithmetic, body(): jnp.sum(grad_heads * padded[:, offset:offset + length], axis=(0, 1))  30.3 us
    psum x1, blocking collectives, body(): grad_gain = lax.psum(lax.psum(gain_part, axis_name='sp'), axis_name='dp')  17 us
    all_to_all x1, waiting for transfers between devices, body(): lax.all_to_all(glu, 'sp', split_axis=2, concat_axis=1, tiled=True)  14.2 us
    all_to_all x1, waiting for transfers between devices, body(): lax.all_to_all(conv_out.astype(jnp.bfloat16), 'sp', split_axis=1, concat_...  13.4 us
  transfers between devices with their start and end apart: 8, of which 5 were waited for; matrix products, arithmetic and copies ran while one was open for 41% of the time, Pallas kernels for 0%

profile of v1, /device:TPU:0, one launch (start us, length us, event | category | flops | bytes accessed | tf_op | source)
XLA Modules:
  0.0 435.8 jit_solution(4021218117244527981)
XLA Ops:
  11.9 12.9 %copy.90 = bf16[1,256,2048]{1,0,2:T(2,128)(2,1)} copy(bf16[1,256,2048]{1,2,0:T(8,128)(2,1)S(1)} %fusion.1) | data formatting | bytes 2097152 | tf_op jit(solution)/shard_map/convert_element_type | solution.py:13
  25.3 11.6 %reduce.17 = bf16[2048,256]{1,0:T(8,128)(2,1)S(1)} reduce(bf16[2048,1,256]{2,1,0:T(2,128)(2,1)} %bitcast.178, bf16[]{:T(256)} %broadcast.201), dimensions={1}, to_apply=%bitcast.161.reduce_sub_computation | reduce | bytes 2097154
  38.6 5.4 %all-to-all-start = ((bf16[4,2,65536]{2,1,0:T(2,128)(2,1)}), bf16[4,2,65536]{2,1,0:T(2,128)(2,1)}, u32[]{:S(2)}, u32[]{:S(2)}) async-start(bf16[4,2,65536]{2,1,0:T(2,128)(2,1)} %reshape.389), calls=%async_computation | async-start | bytes 2097152 | tf_op jit(solution)/shard_map/all_to_all | solution.py:14
  44.1 14.2 %all-to-all-done = bf16[4,2,65536]{2,1,0:T(2,128)(2,1)} async-done(((bf16[4,2,65536]{2,1,0:T(2,128)(2,1)}), bf16[4,2,65536]{2,1,0:T(2,128)(2,1)}, u32[]{:S(2)}, u32[]{:S(2)}) %all-to-all-start) | async-done | bytes 1048608 | tf_op jit(solution)/shard_map/all_to_all | solution.py:14
  64.9 8.0 %add_convert_fusion.1 = bf16[1,1024,512]{2,1,0:T(8,128)(2,1)S(1)} fusion(f32[1,1024,512]{2,1,0:T(8,128)S(1)} %bitcast.163, f32[512]{0:T(512)S(1)} %bitcast.207, f32[512]{0:T(512)S(1)} %bitcast.209, f32[512]{0:T(512)S(1)} %bitcast.213, f32[512]{0:T(512)S(1)} %bitcast.215, f32[512]{0:T(512)S(1)} %bitcast.217, f32[512]{0:T(512)S(1)} %bitcast.219, ...), kind=kLoop, calls=%fused_computation.88 | loop fusion | flops 32505856 | bytes 3209216 | tf_op jit(solution)/shard_map/convert_element_type | solution.py:23
  75.8 8.1 %reduce.18 = bf16[1024,512]{1,0:T(8,128)(2,1)S(1)} reduce(bf16[1024,1,512]{2,1,0:T(2,128)(2,1)} %bitcast.180, bf16[]{:T(256)} %broadcast.201), dimensions={1}, to_apply=%bitcast.160.reduce_sub_computation | reduce | bytes 2097154
  85.9 4.3 all-to-all-start.1
  90.2 13.4 %all-to-all-done.1 = bf16[4,2,65536]{2,1,0:T(2,128)(2,1)} async-done(((bf16[4,2,65536]{2,1,0:T(2,128)(2,1)}), bf16[4,2,65536]{2,1,0:T(2,128)(2,1)}, u32[]{:S(2)}, u32[]{:S(2)}) %all-to-all-start.1) | async-done | bytes 1048608 | tf_op jit(solution)/shard_map/all_to_all | solution.py:22
  117.4 9.3 %convolution_bitcast_fusion = f32[2048,2048]{0,1:T(8,128)} fusion(bf16[256,2048]{0,1:T(8,128)(2,1)} %bitcast.186, bf16[1,256,2048]{2,1,0:T(8,128)(2,1)S(1)} %copy-done), kind=kOutput, calls=%fused_computation | convolution fusion | flops 2147483648 | bytes 18874368 | tf_op jit(solution)/shard_map/dot_general | solution.py:66
  129.0 5.8 %multiply_reduce_fusion = (f32[2048]{0:T(1024)S(1)}, f32[256]{0:T(256)S(1)}, f32[256]{0:T(256)S(1)}, f32[256,2048]{1,0:T(8,128)S(1)}) fusion(f32[256,2048]{1,0:T(8,128)S(1)} %bitcast.176, f32[256]{0:T(256)S(1)} %broadcast_multiply_fusion.2, f32[256]{0:T(256)S(1)} %add_rsqrt_fusion, f32[2048]{0:T(1024)S(1)} %copy-done.13, ...), kind=kOutput, calls=%fused_computation.20 | convolution fusion | flops 2156393984 | bytes 13651968 | tf_op jit(solution)/shard_map/dot_general | solution.py:34
  137.2 11.0 %reduce.19 = bf16[2048,256]{1,0:T(8,128)(2,1)S(1)} reduce(bf16[2048,1,256]{2,1,0:T(2,128)(2,1)S(1)} %bitcast.182, bf16[]{:T(256)} %broadcast.201), dimensions={1}, to_apply=%bitcast.148.reduce_sub_computation | reduce | bytes 2097154
  149.8 3.5 all-to-all-start.2
  153.4 17.0 %psum.29 = f32[2048]{0:T(1024)} all-reduce(f32[2048]{0:T(1024)S(1)} %get-tuple-element.35), channel_id=1, replica_groups=mesh['sp'=4,'dp'=8] {'sp'}, use_global_device_ids=true, to_apply=%region_39.40 | all-reduce | flops 2048 | bytes 16384 | tf_op jit(solution)/shard_map/psum | solution.py:63
  175.3 119.9 %reduce-scatter.2.cloned.1.call-done = f32[256,2048]{0,1:T(8,128)} async-done(((f32[2048,2048]{0,1:T(8,128)}), f32[256,2048]{0,1:T(8,128)}) %reduce-scatter.2.cloned.1.call-update) | async-done | bytes 2097168 | tf_op jit(solution)/shard_map/reduce_scatter | solution.py:65
  295.3 8.0 %add_convert_fusion = bf16[1,1024,512]{2,1,0:T(8,128)(2,1)S(1)} fusion(f32[1,1024,512]{2,1,0:T(8,128)S(1)} %bitcast.162, f32[512]{0:T(512)S(1)} %bitcast.208, f32[512]{0:T(512)S(1)} %bitcast.210, f32[512]{0:T(512)S(1)} %bitcast.214, f32[512]{0:T(512)S(1)} %bitcast.216, f32[512]{0:T(512)S(1)} %bitcast.218, f32[512]{0:T(512)S(1)} %bitcast.220, ...), kind=kLoop, calls=%fused_computation.52 | loop fusion | flops 32505856 | bytes 3209216 | tf_op jit(solution)/shard_map/convert_element_type | solution.py:59
  303.2 2.9 copy.88
  306.2 8.0 %reduce.20 = bf16[1024,512]{1,0:T(8,128)(2,1)S(1)} reduce(bf16[1024,1,512]{2,1,0:T(2,128)(2,1)} %bitcast.179, bf16[]{:T(256)} %broadcast.201), dimensions={1}, to_apply=%bitcast.159.reduce_sub_computation | reduce | bytes 2097154
  316.2 3.7 all-to-all-start.3
  319.9 18.1 %multiply_reduce_fusion.2 = (f32[512]{0:T(512)S(1)}, f32[512]{0:T(512)S(1)}, f32[512]{0:T(512)S(1)}, f32[512]{0:T(512)S(1)}, f32[512]{0:T(512)S(1)}, /*index=5*/...) fusion(f32[1,1024,512]{2,1,0:T(8,128)} %bitcast.164, ...), kind=kLoop, calls=%fused_computation.22 | loop fusion | flops 18865152 | bytes 4231168 | tf_op jit(solution)/shard_map/reduce_sum | solution.py:56
  338.4 11.8 %multiply_reduce_fusion.3 = (f32[512]{0:T(512)S(1)}, f32[512]{0:T(512)S(1)}, f32[512]{0:T(512)S(1)}, f32[512]{0:T(512)S(1)}, f32[512]{0:T(512)S(1)}, /*index=5*/...) fusion(f32[1,1024,512]{2,1,0:T(8,128)} %bitcast.165, ...), kind=kLoop, calls=%fused_computation.23 | loop fusion | flops 12576768 | bytes 4218880 | tf_op jit(solution)/shard_map/reduce_sum | solution.py:56
  355.7 3.0 copy.70
  358.8 3.6 fusion.4
  366.1 7.1 %all-reduce.6.cloned.1.call-done = f32[256,2048]{0,1:T(8,128)} async-done(((f32[256,2048]{0,1:T(8,128)}), f32[256,2048]{0,1:T(8,128)}) %all-reduce.6.cloned.1.call-update) | async-done | bytes 2097168 | tf_op jit(solution)/shard_map/psum | solution.py:73
  376.1 50.3 %all-reduce.8.cloned.1.call-done = (f32[31,512]{1,0:T(8,128)}, f32[2048]{0:T(1024)}) async-done(((f32[31,512]{1,0:T(8,128)}, f32[2048]{0:T(1024)}), (f32[31,512]{1,0:T(8,128)}, f32[2048]{0:T(1024)})) %all-reduce.8.cloned.1.call-update) | async-done | bytes 71696 | tf_op jit(solution)/shard_map/psum | solution.py:57
  (85 shorter events, 60.6 us)
Async XLA Ops:
  7.2 110.3 %copy-start = (bf16[1,256,2048]{2,1,0:T(8,128)(2,1)S(1)}, bf16[1,256,2048]{2,1,0:T(8,128)(2,1)}, u32[]{:S(2)}) copy-start(bf16[1,256,2048]{2,1,0:T(8,128)(2,1)} %param.8) | copy-start | bytes 3145732
  7.2 121.8 %all-gather.2.cloned.1.call-start = ((), (), s32[]{:S(2)}) async-start(), calls=%async_computation.5 | async-start | bytes 9437184 | tf_op jit(solution)/shard_map/all_gather | solution.py:36
  9.4 2.5 copy-start.8
  11.3 13.5 %copy-start.10 = (bf16[1,256,2048]{1,2,0:T(8,128)(2,1)}, bf16[1,256,2048]{1,2,0:T(8,128)(2,1)S(1)}, u32[]{:S(2)}) copy-start(bf16[1,256,2048]{1,2,0:T(8,128)(2,1)S(1)} %copy.57) | copy-start | bytes 3145732
  37.0 7.0 %copy-start.12 = (f32[31,512]{1,0:T(8,128)S(1)}, f32[31,512]{1,0:T(8,128)}, u32[]{:S(2)}) copy-start(f32[31,512]{1,0:T(8,128)} %param.9) | copy-start | bytes 190468
  38.6 19.7 %all-to-all-start = ((bf16[4,2,65536]{2,1,0:T(2,128)(2,1)}), bf16[4,2,65536]{2,1,0:T(2,128)(2,1)}, u32[]{:S(2)}, u32[]{:S(2)}) async-start(bf16[4,2,65536]{2,1,0:T(2,128)(2,1)} %reshape.389), calls=%async_computation | async-start | bytes 2097152 | tf_op jit(solution)/shard_map/all_to_all | solution.py:14
  60.9 2.0 copy-start.3
  64.9 10.9 %copy-start.2 = (f32[1,4,256,512]{3,2,1,0:T(8,128)}, f32[1,4,256,512]{3,2,1,0:T(8,128)S(1)}, u32[]{:S(2)}) copy-start(f32[1,4,256,512]{3,2,1,0:T(8,128)S(1)} %copy.60) | copy-start | bytes 6291460
  83.9 6.3 %copy-start.13 = (f32[2048]{0:T(1024)S(1)}, f32[2048]{0:T(1024)}, u32[]{:S(2)}) copy-start(f32[2048]{0:T(1024)} %param.10) | copy-start | bytes 24580
  85.9 17.7 %all-to-all-start.1 = ((bf16[4,2,65536]{2,1,0:T(2,128)(2,1)}), bf16[4,2,65536]{2,1,0:T(2,128)(2,1)}, u32[]{:S(2)}, u32[]{:S(2)}) async-start(bf16[4,2,65536]{2,1,0:T(2,128)(2,1)} %reshape.391), calls=%async_computation.1 | async-start | bytes 2097152 | tf_op jit(solution)/shard_map/all_to_all | solution.py:22
  90.2 205.1 %reduce-scatter.2.cloned.1.call-start = ((), (), s32[]{:S(2)}) async-start(), calls=%async_computation.6 | async-start | bytes 18874368 | tf_op jit(solution)/shard_map/reduce_scatter | solution.py:65
  106.4 1.3 copy-start.7
  149.8 20.6 %all-to-all-start.2 = ((bf16[4,2,65536]{2,1,0:T(2,128)(2,1)}), bf16[4,2,65536]{2,1,0:T(2,128)(2,1)S(1)}, u32[]{:S(2)}, u32[]{:S(2)}) async-start(bf16[4,2,65536]{2,1,0:T(2,128)(2,1)} %reshape.393), calls=%async_computation.2 | async-start | bytes 2097152 | tf_op jit(solution)/shard_map/all_to_all | solution.py:47
  153.4 219.8 %all-reduce.6.cloned.1.call-start = ((), (), s32[]{:S(2)}) async-start(), calls=%async_computation.7 | async-start | bytes 4194304 | tf_op jit(solution)/shard_map/psum | solution.py:73
  171.4 2.0 copy-start.5
  316.2 36.6 %all-to-all-start.3 = ((bf16[4,2,65536]{2,1,0:T(2,128)(2,1)}), bf16[4,2,65536]{2,1,0:T(2,128)(2,1)S(1)}, u32[]{:S(2)}, u32[]{:S(2)}) async-start(bf16[4,2,65536]{2,1,0:T(2,128)(2,1)} %reshape.395), calls=%async_computation.3 | async-start | bytes 2097152 | tf_op jit(solution)/shard_map/all_to_all | solution.py:58
  319.9 106.4 %all-reduce.8.cloned.1.call-start = ((), (), s32[]{:S(2)}) async-start(), calls=%async_computation.8 | async-start | bytes 147456 | tf_op jit(solution)/shard_map/psum | solution.py:57
  319.9 18.1 %copy-start.4 = (bf16[2048,1,256]{2,1,0:T(2,128)(2,1)S(1)}, bf16[2048,1,256]{2,1,0:T(2,128)(2,1)}, u32[]{:S(2)}) copy-start(bf16[2048,1,256]{2,1,0:T(2,128)(2,1)} %copy-done.3) | copy-start | bytes 3145732
  319.9 18.1 %copy-start.6 = (bf16[2048,1,256]{2,1,0:T(2,128)(2,1)S(1)}, bf16[2048,1,256]{2,1,0:T(2,128)(2,1)}, u32[]{:S(2)}) copy-start(bf16[2048,1,256]{2,1,0:T(2,128)(2,1)} %copy-done.5) | copy-start | bytes 3145732
  355.7 3.0 copy-start.9
  355.7 3.0 copy-start.11
  364.7 64.5 %copy-start.1 = (bf16[1,256,2048]{2,1,0:T(8,128)(2,1)S(1)}, bf16[1,256,2048]{2,1,0:T(8,128)(2,1)}, u32[]{:S(2)}) copy-start(bf16[1,256,2048]{2,1,0:T(8,128)(2,1)} %param.8) | copy-start | bytes 3145732
Sparse Core Ops, SparseCore 0:
  9.6 84.7 all-gather.1
  126.9 168.3 reduce-scatter.1
  298.4 74.7 all-reduce.5
  376.0 50.2 all-reduce.7
